TPU v7x, 32 devices: a whole 2x2x4 slice. The times are simulated.
32 devices in a mesh: ep: 4 (over y, x), tp: 8 (over z, core).
Axes of the slice: x: 2, y: 2, z: 4, core: 2. Of those that a mesh axis runs over, the one named last changes fastest.
Arguments:
- tokens: bfloat16 [1024, 2048], P('ep', 'tp'), may hold values from -600 to 600
- pre_gain: float32 [2048], P('tp'), may hold values from 0.1 to 1.9
- expert_gate: bfloat16 [4, 2048, 8192], P('ep', None, 'tp'), may hold values from -0.125 to 0.125
- expert_up: bfloat16 [4, 2048, 8192], P('ep', None, 'tp'), may hold values from -0.125 to 0.125
- expert_down: bfloat16 [4, 8192, 2048], P('ep', 'tp'), may hold values from -8 to 8
- routes: int32 [1024, 2], P('ep'), may hold values from 0 to 3, all different within a row; in each aligned block of 256 rows (0 to 255, 256 to 511, ...) at most 192 rows name the same one
- route_weights: float32 [1024, 2], P('ep'), may hold values from 0.1 to 1
- post_gain: float32 [2048], P('tp'), may hold values from 0.1 to 1.9
Outputs:
- layer_out: bfloat16 [1024, 2048], P('ep', 'tp')
Inputs may be any that keep to these rules, and one draw needn't show every extreme that they name: `routes`: each token names 2 different experts. Among the 256 tokens of one index of ep no expert is named more than 192 times, a bound that some expert reaches in some of these blocks.
All inputs are finite; a program needn't handle non-finite values.
Results may differ from a plain program's by a relative error of at most 0.024.
Values may be sent and summed in bfloat16 or wider, within the bound.
A program may use at most 64 MiB of HBM per device.

v0:
```python
import jax
import jax.numpy as jnp
from jax import lax
from jax.sharding import PartitionSpec as P

EPSILON = 1e-06


def local(tokens, pre_gain, expert_gate, expert_up, expert_down, routes, route_weights, post_gain):
    local_experts = expert_gate.shape[0]
    groups = lax.axis_size("ep")
    experts_all = local_experts * groups
    tok_rows, part_width = tokens.shape
    full_width = part_width * lax.axis_size("tp")
    capacity = 3 * tok_rows // experts_all
    values = tokens.astype(jnp.float32)
    input_sq = lax.psum(jnp.sum(values * values, axis=-1), "tp")
    normed = (
        values * lax.rsqrt(input_sq / full_width + EPSILON)[:, None] * pre_gain[None, :]
    ).astype(jnp.bfloat16)
    onehot = (routes[:, :, None] == jnp.arange(experts_all, dtype=jnp.int32)).astype(jnp.int32)
    onehot = onehot.reshape(tok_rows * 2, experts_all)
    earlier = jnp.cumsum(onehot, axis=0) - onehot
    slots = jnp.sum(earlier * onehot, axis=-1).reshape(tok_rows, 2)
    positions = routes * capacity + slots
    places = jnp.arange(experts_all * capacity, dtype=jnp.int32)
    first_pick = (places[:, None] == positions[None, :, 0]).astype(jnp.bfloat16)
    second_pick = (places[:, None] == positions[None, :, 1]).astype(jnp.bfloat16)
    dispatch = first_pick + second_pick
    outgoing = jnp.dot(dispatch, normed, preferred_element_type=jnp.float32).astype(jnp.bfloat16)
    arrived = lax.all_to_all(outgoing, "ep", split_axis=0, concat_axis=0, tiled=True)
    fragment = lax.all_gather(arrived, "tp", axis=1, tiled=True)
    count = fragment.shape[1]
    grouped = fragment.reshape(groups, local_experts, capacity, count)
    gate_pre = jnp.einsum(
        "secw,ewf->secf", grouped, expert_gate, preferred_element_type=jnp.float32
    )
    up_pre = jnp.einsum("secw,ewf->secf", grouped, expert_up, preferred_element_type=jnp.float32)
    hidden = (jax.nn.silu(gate_pre) * up_pre).astype(jnp.bfloat16)
    product = jnp.einsum("secf,efd->dsec", hidden, expert_down, preferred_element_type=jnp.float32)
    summed = lax.psum_scatter(
        product.reshape(lax.axis_size("tp") * part_width, groups * local_experts * capacity).astype(
            jnp.bfloat16
        ),
        "tp",
        scatter_dimension=0,
        tiled=True,
    )
    returned = lax.all_to_all(summed, "ep", split_axis=1, concat_axis=1, tiled=True)
    contract = (((0,), (1,)), ((), ()))
    first_out = lax.dot_general(first_pick, returned, contract, preferred_element_type=jnp.float32)
    second_out = lax.dot_general(
        second_pick, returned, contract, preferred_element_type=jnp.float32
    )
    combined = route_weights[:, 0:1] * first_out + route_weights[:, 1:2] * second_out
    output_sq = lax.psum(jnp.sum(combined * combined, axis=-1), "tp")
    scaled = combined * lax.rsqrt(output_sq / full_width + EPSILON)[:, None] * post_gain[None, :]
    return scaled.astype(jnp.bfloat16)


def solution(mesh):
    placed = (
        P("ep", "tp"),
        P("tp"),
        P("ep", None, "tp"),
        P("ep", None, "tp"),
        P("ep", "tp", None),
        P("ep", None),
        P("ep", None),
        P("tp"),
    )
    return jax.shard_map(
        local, mesh=mesh, in_specs=placed, out_specs=P("ep", "tp"), check_vma=False
    )
```

profile of v0, /device:TPU:0, one launch (start us, length us, event | category | flops | bytes accessed | tf_op | source)
XLA Modules:
  0.0 164.0 jit_solution(8557718616161930768)
XLA Ops:
  6.5 0.0 all-gather.2.cloned.1.call-start
  6.5 0.8 copy.20
  7.4 0.1 eq.61
  7.5 0.1 eq.57
  7.7 1.2 reduce-window.6
  8.9 0.2 slice_reduce_fusion
  9.1 0.2 reduce-window.9
  9.3 0.1 add_bitcast_fusion
  9.4 0.1 reshape.55
  9.5 0.1 copy.22
  9.6 0.7 multiply_add_fusion
  10.3 1.0 fusion.28
  11.3 18.1 %psum.14 = f32[256]{0:T(256)S(1)} all-reduce(f32[256]{0:T(256)S(1)} %fusion.28), channel_id=1, replica_groups=mesh['ep'=4,'tp'=8] {'tp'}, use_global_device_ids=true, to_apply=%region_4.5 | all-reduce | flops 256 | bytes 2048 | tf_op jit(solution)/shard_map/psum | solution.py:17
  29.4 1.3 convolution_convert_fusion
  30.7 10.1 %all_to_all.24 = bf16[4,192,256]{2,1,0:T(8,128)(2,1)} all-to-all(bf16[4,192,256]{2,1,0:T(8,128)(2,1)S(1)} %bitcast.82), channel_id=1, replica_groups=mesh['ep'=4,'tp'=8] {'ep'}, dimensions={0} | all-to-all | bytes 786432 | tf_op jit(solution)/shard_map/all_to_all | solution.py:31
  40.8 0.0 all-gather.2.cloned.1.call-update
  40.8 0.0 reduce-scatter.2.cloned.1.call-start
  40.8 35.9 %all-gather.2.cloned.1.call-done = bf16[768,2048]{1,0:T(8,128)(2,1)} async-done(((bf16[768,256]{1,0:T(8,128)(2,1)}), bf16[768,2048]{1,0:T(8,128)(2,1)}) %all-gather.2.cloned.1.call-update) | async-done | bytes 3145744 | tf_op jit(solution)/shard_map/all_gather | solution.py:32
  76.8 6.3 %fusion.2 = f32[4,192,1024]{2,1,0:T(8,128)S(1)} fusion(bf16[4,192,2048]{2,1,0:T(8,128)(2,1)} %bitcast.90, bf16[1,2048,1024]{2,1,0:T(8,128)(2,1)} %param.11), kind=kOutput, calls=%fused_computation.2 | convolution fusion | flops 3221225472 | bytes 10485760 | tf_op jit(solution)/shard_map/secw,ewf->secf/dot_general | solution.py:38
  83.1 0.0 copy-start.3
  83.1 3.8 %fusion.9 = bf16[4,1,192,1024]{3,2,0,1:T(8,128)(2,1)S(1)} fusion(f32[4,192,1024]{2,1,0:T(8,128)S(1)} %fusion.2, bf16[4,192,2048]{2,1,0:T(8,128)(2,1)S(1)} %bitcast.91, bf16[1,2048,1024]{2,1,0:T(8,128)(2,1)S(1)} %copy-done.2), kind=kOutput, calls=%fused_computation.8 | convolution fusion | flops 3225944064 | bytes 12058624 | tf_op jit(solution)/shard_map/secw,ewf->secf/dot_general | solution.py:35
  87.0 4.8 %fusion.13 = bf16[2048,768]{0,1:T(8,128)(2,1)} fusion(bf16[768,1024]{1,0:T(8,128)(2,1)S(1)} %bitcast.92, bf16[1,1024,2048]{2,1,0:T(8,128)(2,1)S(1)} %copy-done.3), kind=kOutput, calls=%fused_computation.14 | convolution fusion | flops 3222798336 | bytes 8912896 | tf_op jit(solution)/shard_map/secf,efd->dsec/dot_general | solution.py:40
  91.8 0.0 reduce-scatter.2.cloned.1.call-update
  91.8 38.8 %reduce-scatter.2.cloned.1.call-done = bf16[256,768]{0,1:T(8,128)(2,1)} async-done(((bf16[2048,768]{0,1:T(8,128)(2,1)}), bf16[256,768]{0,1:T(8,128)(2,1)}) %reduce-scatter.2.cloned.1.call-update) | async-done | bytes 393232 | tf_op jit(solution)/shard_map/reduce_scatter | solution.py:41
  130.6 3.6 %all-to-all-start.1 = ((bf16[256,4,192]{0,2,1:T(8,128)(2,1)}), bf16[256,4,192]{0,2,1:T(8,128)(2,1)S(1)}, u32[]{:S(2)}, u32[]{:S(2)}) async-start(bf16[256,4,192]{0,2,1:T(8,128)(2,1)} %bitcast.81), calls=%async_computation.2 | async-start | bytes 786432 | tf_op jit(solution)/shard_map/all_to_all | solution.py:49
  134.2 5.9 %all-to-all-done.1 = bf16[256,4,192]{0,2,1:T(8,128)(2,1)S(1)} async-done(((bf16[256,4,192]{0,2,1:T(8,128)(2,1)}), bf16[256,4,192]{0,2,1:T(8,128)(2,1)S(1)}, u32[]{:S(2)}, u32[]{:S(2)}) %all-to-all-start.1) | async-done | bytes 393248 | tf_op jit(solution)/shard_map/all_to_all | solution.py:49
  140.1 0.4 convolution_multiply_fusion.1
  140.5 0.4 multiply_reduce_fusion
  140.9 15.4 %psum.15 = f32[256]{0:T(256)S(1)} all-reduce(f32[256]{0:T(256)S(1)} %get-tuple-element.9), channel_id=1, replica_groups=mesh['ep'=4,'tp'=8] {'tp'}, use_global_device_ids=true, to_apply=%region_7.8 | all-reduce | flops 256 | bytes 2048 | tf_op jit(solution)/shard_map/psum | solution.py:56
  156.3 0.0 copy-done.1
  156.3 0.1 multiply_convert_fusion
  156.4 0.8 copy.23
  (14 shorter events, 0.1 us)
Async XLA Ops:
  6.5 70.3 %all-gather.2.cloned.1.call-start = ((), (), s32[]{:S(2)}) async-start(), calls=%async_computation.3 | async-start | bytes 3538944 | tf_op jit(solution)/shard_map/all_gather | solution.py:32
  40.8 89.8 %reduce-scatter.2.cloned.1.call-start = ((), (), s32[]{:S(2)}) async-start(), calls=%async_computation.4 | async-start | bytes 3538944 | tf_op jit(solution)/shard_map/reduce_scatter | solution.py:41
  76.8 6.3 %copy-start.2 = (bf16[1,2048,1024]{2,1,0:T(8,128)(2,1)S(1)}, bf16[1,2048,1024]{2,1,0:T(8,128)(2,1)}, u32[]{:S(2)}) copy-start(bf16[1,2048,1024]{2,1,0:T(8,128)(2,1)} %param.10) | copy-start | bytes 12582916
  76.8 6.3 %copy-start.4 = (bf16[768,2048]{1,0:T(8,128)(2,1)S(1)}, bf16[768,2048]{1,0:T(8,128)(2,1)}, u32[]{:S(2)}) copy-start(bf16[768,2048]{1,0:T(8,128)(2,1)} %all-gather.2.cloned.1.call-done) | copy-start | bytes 9437188
  83.1 3.9 %copy-start.3 = (bf16[1,1024,2048]{2,1,0:T(8,128)(2,1)S(1)}, bf16[1,1024,2048]{2,1,0:T(8,128)(2,1)}, u32[]{:S(2)}) copy-start(bf16[1,1024,2048]{2,1,0:T(8,128)(2,1)} %param.12) | copy-start | bytes 12582916
  91.8 42.4 %copy-start = (f32[256,2]{0,1:T(2,128)S(1)}, f32[256,2]{0,1:T(2,128)}, u32[]{:S(2)}) copy-start(f32[256,2]{0,1:T(2,128)} %param.14) | copy-start | bytes 6148
  91.8 64.5 %copy-start.1 = (f32[256]{0:T(256)S(1)}, f32[256]{0:T(256)}, u32[]{:S(2)}) copy-start(f32[256]{0:T(256)} %param.15) | copy-start | bytes 3076
  130.6 9.5 %all-to-all-start.1 = ((bf16[256,4,192]{0,2,1:T(8,128)(2,1)}), bf16[256,4,192]{0,2,1:T(8,128)(2,1)S(1)}, u32[]{:S(2)}, u32[]{:S(2)}) async-start(bf16[256,4,192]{0,2,1:T(8,128)(2,1)} %bitcast.81), calls=%async_computation.2 | async-start | bytes 786432 | tf_op jit(solution)/shard_map/all_to_all | solution.py:49
Sparse Core Ops, SparseCore 0:
  40.9 35.8 all-gather.1
  91.9 38.5 reduce-scatter.1
where the time goes:
time: 164 us
  waiting for transfers between devices  80.6 us (49%)
  blocking collectives  43.6 us (27%)
  matrix products  17 us (10%)
  between operations  13.5 us (8%)
  starting transfers between devices  3.69 us (2%)
  other arithmetic  3.35 us (2%)
  local copies, waits for them, and re-layouts  2.31 us (1%)
    reduce_scatter x1, waiting for transfers between devices, local(): lax.psum_scatter(product.reshape(lax.axis_size('tp') * part_width, groups...  38.8 us
    all_gather x1, waiting for transfers between devices, local(): fragment = lax.all_gather(arrived, 'tp', axis=1, tiled=True)  35.9 us
    psum x1, blocking collectives, local(): input_sq = lax.psum(jnp.sum(values * values, axis=-1), 'tp')  18.1 us
    psum x1, blocking collectives, local(): output_sq = lax.psum(jnp.sum(combined * combined, axis=-1), 'tp')  15.4 us
    all_to_all x1, blocking collectives, local(): lax.all_to_all(outgoing, 'ep', split_axis=0, concat_axis=0, tiled=True)  10.1 us
    dot_general x1, matrix products, local(): jnp.einsum('secw,ewf->secf', grouped, expert_up, preferred_element_type=j...  6.28 us
    all_to_all x1, waiting for transfers between devices, local(): lax.all_to_all(summed, 'ep', split_axis=1, concat_axis=1, tiled=True)  5.87 us
    dot_general x1, matrix products, local(): jnp.einsum('secf,efd->dsec', hidden, expert_down, preferred_element_type=...  4.83 us
  transfers between devices with their start and end apart: 3, of which 3 were waited for; matrix products, arithmetic and copies ran while one was open for 0% of the time, Pallas kernels for 0%

commit v1 on v0

--- a/solution.py
+++ b/solution.py
@@ -4,6 +4,28 @@
 from jax.sharding import PartitionSpec as P
 
 EPSILON = 1e-06
+
+
+def in_order(pieces, dim):
+    pieces = jnp.moveaxis(pieces, 0, dim)
+    dims = pieces.shape
+    return pieces.reshape(*dims[:dim], dims[dim] * dims[dim + 1], *dims[dim + 2 :])
+
+
+def doubled(x, axis):
+    size = lax.axis_size(axis)
+    blocks = x[None]
+    for level in range(size.bit_length() - 1):
+        apart = 1 << level
+        other = lax.ppermute(blocks, axis, [(i, i ^ apart) for i in range(size)])
+        both = jnp.stack([blocks, other])
+        upper = lax.axis_index(axis) >> level & 1
+        blocks = jnp.where(upper == 0, both, both[::-1]).reshape(-1, *x.shape)
+    return blocks
+
+
+def gather_by_bits(array, axis, dim):
+    return in_order(doubled(array, axis), dim)
 
 
 def local(tokens, pre_gain, expert_gate, expert_up, expert_down, routes, route_weights, post_gain):
@@ -29,7 +51,7 @@
     dispatch = first_pick + second_pick
     outgoing = jnp.dot(dispatch, normed, preferred_element_type=jnp.float32).astype(jnp.bfloat16)
     arrived = lax.all_to_all(outgoing, "ep", split_axis=0, concat_axis=0, tiled=True)
-    fragment = lax.all_gather(arrived, "tp", axis=1, tiled=True)
+    fragment = gather_by_bits(arrived, "tp", 1)
     count = fragment.shape[1]
     grouped = fragment.reshape(groups, local_experts, capacity, count)
     gate_pre = jnp.einsum(

time: 164 us -> 232 us (1.41)
  waiting for transfers between devices: 80.6 us -> 133 us
  local copies, waits for them, and re-layouts: 2.31 us -> 12 us
  other arithmetic: 3.35 us -> 9.15 us
    ppermute x0 -> x3, waiting for transfers between devices: none -> 90.3 us  [doubled(): other = lax.ppermute(blocks, axis, [(i, i ^ apart) for i in range(size)])]
    all_gather x1 -> x0, waiting for transfers between devices: 35.9 us -> none  [local(): fragment = lax.all_gather(arrived, 'tp', axis=1, tiled=True)]
    another operation x0 -> x2, local copies, waits for them, and re-layouts: none -> 5.41 us
    reshape x0 -> x2, local copies, waits for them, and re-layouts: none -> 4.24 us  [doubled(): blocks = jnp.where(upper == 0, both, both[::-1]).reshape(-1, *x.shape)]
    another operation x2 -> x6, other arithmetic: 1.41 us -> 5.25 us  [the longest x4 3.85 us: doubled(): both = jnp.stack([blocks, other])]
  transfers between devices with their start and end apart: 3 -> 5, of which waited for: 3 -> 5; matrix products, arithmetic and copies ran while one was open for 0% -> 1% of each run, Pallas kernels for 0% -> 0%
where the time goes in v1:
time: 232 us
  waiting for transfers between devices  133 us (57%)
  blocking collectives  43.4 us (19%)
  matrix products  16.2 us (7%)
  between operations  13.6 us (6%)
  local copies, waits for them, and re-layouts  12 us (5%)
  other arithmetic  9.15 us (4%)
  starting transfers between devices  3.78 us (2%)
    ppermute x3, waiting for transfers between devices, doubled(): other = lax.ppermute(blocks, axis, [(i, i ^ apart) for i in range(size)])  90.3 us
    reduce_scatter x1, waiting for transfers between devices, local(): lax.psum_scatter(product.reshape(lax.axis_size('tp') * part_width, groups...  37.2 us
    psum x1, blocking collectives, local(): input_sq = lax.psum(jnp.sum(values * values, axis=-1), 'tp')  18.1 us
    psum x1, blocking collectives, local(): output_sq = lax.psum(jnp.sum(combined * combined, axis=-1), 'tp')  15.4 us
    all_to_all x1, blocking collectives, local(): lax.all_to_all(outgoing, 'ep', split_axis=0, concat_axis=0, tiled=True)  9.94 us
    all_to_all x1, waiting for transfers between devices, local(): lax.all_to_all(summed, 'ep', split_axis=1, concat_axis=1, tiled=True)  5.87 us
    dot_general x1, matrix products, local(): jnp.einsum('secw,ewf->secf', grouped, expert_up, preferred_element_type=j...  5.35 us
    dot_general x1, matrix products, local(): jnp.einsum('secf,efd->dsec', hidden, expert_down, preferred_element_type=...  5.01 us
  transfers between devices with their start and end apart: 5, of which 5 were waited for; matrix products, arithmetic and copies ran while one was open for 1% of the time, Pallas kernels for 0%

profile of v1, /device:TPU:0, one launch (start us, length us, event | category | flops | bytes accessed | tf_op | source)
XLA Modules:
  0.0 231.6 jit_solution(14586982678000928809)
XLA Ops:
  6.5 0.8 copy.26
  7.4 0.1 eq.70
  7.7 1.2 reduce-window.6
  8.9 0.2 slice_reduce_fusion
  9.1 0.2 reduce-window.9
  9.6 0.7 multiply_add_fusion
  10.3 1.0 fusion.30
  11.3 18.1 %psum.14 = f32[256]{0:T(256)S(1)} all-reduce(f32[256]{0:T(256)S(1)} %fusion.30), channel_id=1, replica_groups=mesh['ep'=4,'tp'=8] {'tp'}, use_global_device_ids=true, to_apply=%region_4.5 | all-reduce | flops 256 | bytes 2048 | tf_op jit(solution)/shard_map/psum | solution.py:39
  29.4 1.3 convolution_convert_fusion
  30.7 9.9 %all_to_all.21 = bf16[4,192,256]{2,1,0:T(8,128)(2,1)S(1)} all-to-all(bf16[4,192,256]{2,1,0:T(8,128)(2,1)S(1)} %bitcast.99), channel_id=1, replica_groups=mesh['ep'=4,'tp'=8] {'ep'}, dimensions={0} | all-to-all | bytes 786432 | tf_op jit(solution)/shard_map/all_to_all | solution.py:53
  40.7 1.7 collective-permute-done
  42.5 0.2 fusion.22
  42.8 19.6 %collective-permute-done.1 = bf16[2,768,256]{2,1,0:T(8,128)(2,1)S(1)} collective-permute-done((bf16[2,768,256]{2,1,0:T(8,128)(2,1)S(1)}, bf16[2,768,256]{2,1,0:T(8,128)(2,1)S(1)}, u32[]{:S(2)}, u32[]{:S(2)}) %collective-permute-start.1) | collective-permute-done | bytes 786464 | tf_op jit(solution)/shard_map/ppermute | solution.py:20
  62.3 0.1 pad_maximum_fusion.1
  62.5 0.3 reverse_select_fusion.1
  62.8 1.2 copy.29
  64.1 1.2 copy.30
  65.3 69.0 %collective-permute-done.2 = bf16[4,768,256]{2,0,1:T(4,128)(2,1)} collective-permute-done((bf16[4,768,256]{2,0,1:T(4,128)(2,1)S(1)}, bf16[4,768,256]{2,0,1:T(4,128)(2,1)}, u32[]{:S(2)}, u32[]{:S(2)}) %collective-permute-start.2) | collective-permute-done | bytes 1572896 | tf_op jit(solution)/shard_map/ppermute | solution.py:20
  134.4 3.4 %pad_maximum_fusion = bf16[2,4,768,256]{3,1,0,2:T(4,128)(2,1)S(1)} fusion(bf16[1,4,768,256]{3,1,0,2:T(4,128)(2,1)} %bitcast.13, bf16[1,4,768,256]{3,1,0,2:T(4,128)(2,1)S(1)} %copy.30), kind=kLoop, calls=%fused_computation.8 | loop fusion | flops 1572864 | bytes 6291456 | tf_op jit(solution)/shard_map/stack | solution.py:21
  137.8 1.6 reverse_select_fusion
  139.4 3.0 %reshape.68 = bf16[8,768,256]{2,0,1:T(8,128)(2,1)} reshape(bf16[2,4,768,256]{3,1,0,2:T(4,128)(2,1)S(1)} %reverse_select_fusion) | data formatting | bytes 6291456 | tf_op jit(solution)/shard_map/reshape | solution.py:23
  142.5 4.2 %reshape.69 = bf16[4,192,2048]{2,1,0:T(8,128)(2,1)S(1)} reshape(bf16[768,8,256]{2,1,0:T(8,128)(2,1)} %bitcast.92) | data formatting | bytes 6291456 | tf_op jit(solution)/shard_map/reshape.4
  146.7 5.3 %fusion.2 = f32[4,192,1024]{2,1,0:T(8,128)S(1)} fusion(bf16[4,192,2048]{2,1,0:T(8,128)(2,1)S(1)} %reshape.69, bf16[1,2048,1024]{2,1,0:T(8,128)(2,1)} %param.11), kind=kOutput, calls=%fused_computation.3 | convolution fusion | flops 3221225472 | bytes 10485760 | tf_op jit(solution)/shard_map/secw,ewf->secf/dot_general | solution.py:60
  152.1 3.8 %fusion.9 = bf16[4,1,192,1024]{3,2,0,1:T(8,128)(2,1)S(1)} fusion(f32[4,192,1024]{2,1,0:T(8,128)S(1)} %fusion.2, bf16[4,192,2048]{2,1,0:T(8,128)(2,1)S(1)} %reshape.69, bf16[1,2048,1024]{2,1,0:T(8,128)(2,1)S(1)} %copy-done.2), kind=kOutput, calls=%fused_computation.10 | convolution fusion | flops 3225944064 | bytes 12058624 | tf_op jit(solution)/shard_map/secw,ewf->secf/dot_general | solution.py:57
  155.9 5.0 %fusion.13 = bf16[2048,768]{0,1:T(8,128)(2,1)} fusion(bf16[768,1024]{1,0:T(8,128)(2,1)S(1)} %bitcast.108, bf16[1,1024,2048]{2,1,0:T(8,128)(2,1)S(1)} %copy-done.3), kind=kOutput, calls=%fused_computation.16 | convolution fusion | flops 3222798336 | bytes 8912896 | tf_op jit(solution)/shard_map/secf,efd->dsec/dot_general | solution.py:62
  161.0 37.2 %reduce-scatter.2.cloned.1.call-done = bf16[256,768]{0,1:T(8,128)(2,1)} async-done(((bf16[2048,768]{0,1:T(8,128)(2,1)}), bf16[256,768]{0,1:T(8,128)(2,1)}) %reduce-scatter.2.cloned.1.call-update) | async-done | bytes 393232 | tf_op jit(solution)/shard_map/reduce_scatter | solution.py:63
  198.2 3.6 %all-to-all-start.1 = ((bf16[256,4,192]{0,2,1:T(8,128)(2,1)}), bf16[256,4,192]{0,2,1:T(8,128)(2,1)S(1)}, u32[]{:S(2)}, u32[]{:S(2)}) async-start(bf16[256,4,192]{0,2,1:T(8,128)(2,1)} %bitcast.98), calls=%async_computation.2 | async-start | bytes 786432 | tf_op jit(solution)/shard_map/all_to_all | solution.py:71
  201.8 5.9 %all-to-all-done.1 = bf16[256,4,192]{0,2,1:T(8,128)(2,1)S(1)} async-done(((bf16[256,4,192]{0,2,1:T(8,128)(2,1)}), bf16[256,4,192]{0,2,1:T(8,128)(2,1)S(1)}, u32[]{:S(2)}, u32[]{:S(2)}) %all-to-all-start.1) | async-done | bytes 393248 | tf_op jit(solution)/shard_map/all_to_all | solution.py:71
  207.7 0.4 convolution_multiply_fusion.1
  208.1 0.4 multiply_reduce_fusion
  208.4 15.4 %psum.15 = f32[256]{0:T(256)S(1)} all-reduce(f32[256]{0:T(256)S(1)} %get-tuple-element.11), channel_id=1, replica_groups=mesh['ep'=4,'tp'=8] {'tp'}, use_global_device_ids=true, to_apply=%region_7.8 | all-reduce | flops 256 | bytes 2048 | tf_op jit(solution)/shard_map/psum | solution.py:78
  224.0 0.8 copy.31
  (25 shorter events, 0.9 us)
Async XLA Ops:
  6.5 191.6 %reduce-scatter.2.cloned.1.call-start = ((), (), s32[]{:S(2)}) async-start(), calls=%async_computation.3 | async-start | bytes 3538944 | tf_op jit(solution)/shard_map/reduce_scatter | solution.py:63
  40.7 1.7 collective-permute-start
  42.7 19.6 %collective-permute-start.1 = (bf16[2,768,256]{2,1,0:T(8,128)(2,1)S(1)}, bf16[2,768,256]{2,1,0:T(8,128)(2,1)S(1)}, u32[]{:S(2)}, u32[]{:S(2)}) collective-permute-start(bf16[2,768,256]{2,1,0:T(8,128)(2,1)S(1)} %get-tuple-element.6), channel_id=1, source_target_pairs={{0,2},{1,3},{2,0},{3,1},{4,6},{5,7},{6,4},{7,5},{8,10},{9,11},{10,... | collective-permute-start | bytes 2359304 | tf_op jit(solution)/shard_map/ppermute | solution.py:20
  64.0 70.4 %collective-permute-start.2 = (bf16[4,768,256]{2,0,1:T(4,128)(2,1)S(1)}, bf16[4,768,256]{2,0,1:T(4,128)(2,1)}, u32[]{:S(2)}, u32[]{:S(2)}) collective-permute-start(bf16[4,768,256]{2,0,1:T(4,128)(2,1)S(1)} %copy.29), channel_id=1, source_target_pairs={{0,4},{1,5},{2,6},{3,7},{4,0},{5,1},{6,2},{7,3},{8,12},{9,13},{10,... | collective-permute-start | bytes 4718600 | tf_op jit(solution)/shard_map/ppermute | solution.py:20
  146.7 5.4 %copy-start.2 = (bf16[1,2048,1024]{2,1,0:T(8,128)(2,1)S(1)}, bf16[1,2048,1024]{2,1,0:T(8,128)(2,1)}, u32[]{:S(2)}) copy-start(bf16[1,2048,1024]{2,1,0:T(8,128)(2,1)} %param.10) | copy-start | bytes 12582916
  152.1 3.9 %copy-start.3 = (bf16[1,1024,2048]{2,1,0:T(8,128)(2,1)S(1)}, bf16[1,1024,2048]{2,1,0:T(8,128)(2,1)}, u32[]{:S(2)}) copy-start(bf16[1,1024,2048]{2,1,0:T(8,128)(2,1)} %param.12) | copy-start | bytes 12582916
  160.9 40.9 %copy-start = (f32[256,2]{0,1:T(2,128)S(1)}, f32[256,2]{0,1:T(2,128)}, u32[]{:S(2)}) copy-start(f32[256,2]{0,1:T(2,128)} %param.14) | copy-start | bytes 6148
  160.9 62.9 %copy-start.1 = (f32[256]{0:T(256)S(1)}, f32[256]{0:T(256)}, u32[]{:S(2)}) copy-start(f32[256]{0:T(256)} %param.15) | copy-start | bytes 3076
  198.2 9.5 %all-to-all-start.1 = ((bf16[256,4,192]{0,2,1:T(8,128)(2,1)}), bf16[256,4,192]{0,2,1:T(8,128)(2,1)S(1)}, u32[]{:S(2)}, u32[]{:S(2)}) async-start(bf16[256,4,192]{0,2,1:T(8,128)(2,1)} %bitcast.98), calls=%async_computation.2 | async-start | bytes 786432 | tf_op jit(solution)/shard_map/all_to_all | solution.py:71
Sparse Core Ops, SparseCore 0:
  161.1 37.0 reduce-scatter.1
